TPU v7x, 32 devices: a whole 2x2x4 slice. The times are simulated.
32 devices in a mesh: sp: 8 (over z, y), tp: 4 (over x, core).
Axes of the slice: x: 2, y: 2, z: 4, core: 2. Of those that a mesh axis runs over, the one named last changes fastest.
Arguments:
- tokens: bfloat16 [2048, 2048], P('sp', 'tp'), may hold values from -19 to 250
- in_gain: bfloat16 [2048], replicated, may hold values from 0.099609375 to 1.8984375
- w_glu_value: bfloat16 [2048, 512], P(None, 'tp'), may hold values from -0.125 to 0.125
- w_glu_gate: bfloat16 [2048, 512], P(None, 'tp'), may hold values from -0.125 to 0.125
- w_query: bfloat16 [2048, 1024], P(None, 'tp'), may hold values from -1 to 1
- w_key: bfloat16 [2048, 512], P(None, 'tp'), may hold values from -1 to 1
- w_value: bfloat16 [2048, 512], P(None, 'tp'), may hold values from -0.125 to 0.125
- w_gate_conv: bfloat16 [2048, 512], P(None, 'tp'), may hold values from -0.125 to 0.125
- w_gate_attn: bfloat16 [2048, 1024], P(None, 'tp'), may hold values from -0.125 to 0.125
- conv_weight: bfloat16 [31, 512], P(None, 'tp'), may hold values from -4.6 to 4.6
- conv_gain: float32 [512], P('tp'), may hold values from 0.1 to 1.9
- lam: float32 [8], P('tp'), may hold values from 0.3 to 0.8
- head_gain: float32 [128], replicated, may hold values from 0.1 to 1.9
- out_conv: bfloat16 [512, 2048], P('tp'), may hold values from -0.15625 to 0.15625
- out_attn: bfloat16 [1024, 2048], P('tp'), may hold values from -0.15625 to 0.15625
Outputs:
- mixed: bfloat16 [2048, 2048], P(('sp', 'tp'))
All inputs are finite; a program needn't handle non-finite values.
Results may differ from a plain program's by a relative error of at most 0.017.
The roundings to bfloat16 on the way count: a program that leaves them out, or rounds other values in their place, can miss the bound.
Values may be sent and summed in bfloat16 or wider, within the bound.
A program may use at most 128 MiB of HBM per device.

v0:
```python
import math
import jax
import jax.numpy as jnp
from jax import lax
from jax.sharding import PartitionSpec as P

D = 2048
CONV = 512
QK = 64
VDIM = 128
WIDTH = 31
EPSILON = 1e-06
NEG_BIG = -1e30
HEAD_SCALE = 0.8


def shifted(x, axis, by):
    count = lax.axis_size(axis)
    pairs = [(i, i + by) for i in range(count) if 0 <= i + by < count]
    return lax.ppermute(x, axis, pairs)


def local(
    tokens,
    in_gain,
    w_glu_value,
    w_glu_gate,
    w_query,
    w_key,
    w_value,
    w_gate_conv,
    w_gate_attn,
    conv_weight,
    conv_gain,
    lam,
    head_gain,
    out_conv,
    out_attn,
):
    tok_rows = tokens.shape[0]
    weights = (w_glu_value, w_glu_gate, w_query, w_key, w_value, w_gate_conv, w_gate_attn)
    widened = lax.all_gather(tokens, "tp", axis=1, tiled=True).astype(jnp.float32)
    gain_part = in_gain.astype(jnp.float32)
    scaled = (widened * gain_part[None, :]).astype(jnp.bfloat16)
    updated = tuple(
        (jnp.dot(scaled, weight, preferred_element_type=jnp.float32) for weight in weights)
    )
    squares = jnp.sum(widened * widened, axis=1)
    inv_rms = lax.rsqrt(squares / D + EPSILON)[:, None]
    glu_value, glu_gate, query, key, value, gate_conv, gate_attn = [
        (total * inv_rms).astype(jnp.bfloat16) for total in updated
    ]
    glued = (glu_value.astype(jnp.float32) * jax.nn.sigmoid(glu_gate.astype(jnp.float32))).astype(
        jnp.bfloat16
    )
    tail_rows = WIDTH - 1
    last_rows = glued[tok_rows - tail_rows :]
    conv_local = glued.shape[1]
    kv_local = key.shape[1] // (2 * QK)
    heads_local = lam.shape[0]
    group = heads_local // kv_local
    my_index = lax.axis_index("sp")
    my_start = my_index * tok_rows
    scale_factor = 1.0 / math.sqrt(QK)
    query_groups = [
        (
            query.reshape(tok_rows, kv_local, group, 2, QK),
            my_start + jnp.arange(tok_rows, dtype=jnp.int32),
        )
    ]
    start_attn = tuple(
        (
            (
                jnp.full((kv_local, group, 2, rows_of.shape[0]), NEG_BIG, jnp.float32),
                jnp.zeros((kv_local, group, 2, rows_of.shape[0]), jnp.float32),
                jnp.zeros((kv_local, group, 2, rows_of.shape[0], VDIM), jnp.float32),
            )
            for rows_of, unused_pos in query_groups
        )
    )
    key_piece = lax.all_gather(key, "sp", axis=0, tiled=True)
    value_piece = lax.all_gather(value, "sp", axis=0, tiled=True)
    shards = key_piece.shape[0] // tok_rows
    stacked_keys = key_piece.reshape(shards, tok_rows, kv_local, 2, QK)
    stacked_values = value_piece.reshape(shards, tok_rows, kv_local, VDIM)
    firsts = tok_rows * jnp.arange(shards, dtype=jnp.int32)

    def visit(states, inputs):
        key_shard, value_shard, first = inputs
        key_pos = first + jnp.arange(tok_rows, dtype=jnp.int32)
        updated_states = []
        for (query_rows, query_pos), current_state in zip(query_groups, states):

            def update(current, query_rows=query_rows, query_pos=query_pos):
                maxima, totals, summed = current
                scores = (
                    jnp.einsum(
                        "qagcd,kacd->agcqk",
                        query_rows,
                        key_shard,
                        preferred_element_type=jnp.float32,
                    )
                    * scale_factor
                )
                allowed = key_pos[None, :] <= query_pos[:, None]
                scores = jnp.where(allowed, scores, NEG_BIG)
                new_max = jnp.maximum(maxima, jnp.max(scores, axis=4))
                factor = jnp.exp(maxima - new_max)
                expd = jnp.exp(scores - new_max[..., None])
                totals = totals * factor + jnp.sum(expd, axis=4)
                summed = summed * factor[..., None] + jnp.einsum(
                    "agcqk,kav->agcqv",
                    expd.astype(jnp.bfloat16),
                    value_shard,
                    preferred_element_type=jnp.float32,
                )
                return (new_max, totals, summed)

            def keep(current):
                return current

            query_last = query_pos[0] + query_pos.shape[0] - 1
            updated_states.append(lax.cond(first <= query_last, update, keep, current_state))
        return (tuple(updated_states), None)

    result, unused = lax.scan(visit, start_attn, (stacked_keys, stacked_values, firsts))
    states = result
    maxima, totals, summed = states[0]
    output = (
        summed[:, :, 0] / totals[:, :, 0][..., None]
        - lam.reshape(kv_local, group)[:, :, None, None]
        * summed[:, :, 1]
        / totals[:, :, 1][..., None]
    )
    normed = output * lax.rsqrt(jnp.mean(output * output, axis=3, keepdims=True) + EPSILON)
    normed = normed * head_gain[None, None, None, :] * HEAD_SCALE
    laid = jnp.transpose(normed, (2, 0, 1, 3)).reshape(normed.shape[2], heads_local * VDIM)
    y_attn = (laid * jax.nn.silu(gate_attn.astype(jnp.float32))).astype(jnp.bfloat16)
    previous = shifted(last_rows, "sp", 1)
    padded = jnp.concatenate([previous, glued], axis=0).astype(jnp.float32)
    taps = conv_weight.astype(jnp.float32)
    conv = jnp.zeros((tok_rows, conv_local), jnp.float32)
    for offset in range(WIDTH):
        conv = conv + padded[offset : offset + tok_rows] * taps[offset][None, :]
    total_sq = lax.psum(jnp.sum(conv * conv, axis=1), "tp")
    normed = conv * lax.rsqrt(total_sq / CONV + EPSILON)[:, None] * conv_gain[None, :]
    y_conv = (jax.nn.silu(normed) * jax.nn.silu(gate_conv.astype(jnp.float32))).astype(jnp.bfloat16)
    return lax.psum_scatter(
        (
            jnp.dot(y_conv, out_conv, preferred_element_type=jnp.float32)
            + jnp.dot(y_attn, out_attn, preferred_element_type=jnp.float32)
        ).astype(jnp.bfloat16),
        "tp",
        scatter_dimension=0,
        tiled=True,
    )


def solution(mesh):
    in_specs = (
        P("sp", "tp"),
        P(),
        P(None, "tp"),
        P(None, "tp"),
        P(None, "tp"),
        P(None, "tp"),
        P(None, "tp"),
        P(None, "tp"),
        P(None, "tp"),
        P(None, "tp"),
        P("tp"),
        P("tp"),
        P(),
        P("tp", None),
        P("tp", None),
    )
    out_specs = P(("sp", "tp"), None)
    return jax.shard_map(local, mesh=mesh, in_specs=in_specs, out_specs=out_specs, check_vma=False)
```

profile of v0, /device:TPU:0, one launch (start us, length us, event | category | flops | bytes accessed | tf_op | source)
XLA Modules:
  0.0 186.6 jit_solution(6918326451705439415)
XLA Ops:
  6.5 0.7 all-gather.2.cloned.1.call-update
  7.3 0.7 convert_element_type.71
  8.5 0.7 convert_element_type.79
  9.8 18.6 %all-gather.2.cloned.1.call-done = bf16[256,2048]{1,0:T(8,128)(2,1)} async-done(((bf16[256,512]{1,0:T(8,128)(2,1)}), bf16[256,2048]{1,0:T(8,128)(2,1)}) %all-gather.2.cloned.1.call-update) | async-done | bytes 1048592 | tf_op jit(solution)/shard_map/all_gather | solution.py:42
  28.3 1.5 fusion.19
  29.9 1.8 fusion.35
  31.7 33.5 %all_gather.10 = bf16[2048,128]{1,0:T(8,128)(2,1)} all-gather(bf16[256,128]{1,0:T(8,128)(2,1)S(1)} %fusion.35), channel_id=1, replica_groups=mesh['sp'=8,'tp'=4] {'sp'}, dimensions={0}, use_global_device_ids=true | all-gather | bytes 589824 | tf_op jit(solution)/shard_map/all_gather | solution.py:81
  65.2 2.4 %reshape.159 = bf16[8,256,1,2,64]{4,3,1,0,2:T(2,128)(2,1)S(1)} reshape(bf16[2048,128]{1,0:T(8,128)(2,1)} %all_gather.10) | data formatting | bytes 1048576 | tf_op jit(solution)/shard_map/reshape | solution.py:84
  67.6 1.8 copy.27
  69.4 1.6 fusion.36
  70.9 31.3 %all_gather.11 = bf16[2048,128]{1,0:T(8,128)(2,1)S(1)} all-gather(bf16[256,128]{1,0:T(8,128)(2,1)S(1)} %fusion.36), channel_id=1, replica_groups=mesh['sp'=8,'tp'=4] {'sp'}, dimensions={0}, use_global_device_ids=true | all-gather | bytes 589824 | tf_op jit(solution)/shard_map/all_gather | solution.py:82
  102.2 0.6 fusion.20
  102.9 13.8 %while.17 = (s32[]{:T(128)}, f32[1,2,2,256]{3,1,2,0:T(2,128)S(1)}, f32[1,2,2,256]{3,1,2,0:T(2,128)S(1)}, f32[1,2,2,256,128]{4,3,2,1,0:T(8,128)S(1)}, s32[8]{0:T(...) while((s32[]{:T(128)}, f32[1,2,2,256]{3,1,2,0:T(2,128)S(1)}, ...), condition=%wide.region_8.9_spmd.clone, body=%wide.region_3.8_spmd.clone.sunk | while | flops 102567424 | bytes 4665123 | solution.py:126
  102.9 0.7 dynamic_slice.38
  104.3 2.8 %conditional.3 = ((f32[1,2,2,256]{3,1,2,0:T(2,128)S(1)}, f32[1,2,2,256]{3,1,2,0:T(2,128)S(1)}, f32[1,2,2,256,128]{4,3,2,1,0:T(8,128)S(1)})) conditional(s32[]{:T(128)} %convert_element_type.190, (f32[1,2,2,256]{3,1,2,0:T(2,128)S(1)}, f32[1,2,2,256]{3,1,2,0:T(2,128)S(1)}, f32[1,2,2,256,128]{4,3,2,1,0:T(8,128)S(1)}) %tuple.82, (s32[]{:T(128)}, ...), branch_computations={%region_4.4_spmd, %region_5.7_spmd} | conditional | flops 102567424 | bytes 4663852 | solution.py:123
  104.3 0.7 broadcast_add_fusion
  105.1 1.2 fusion.99
  107.1 0.7 dynamic_slice.38
  108.5 0.7 dynamic_slice.38
  109.8 0.7 dynamic_slice.38
  111.2 0.7 dynamic_slice.38
  112.6 0.7 dynamic_slice.38
  114.0 0.7 dynamic_slice.38
  115.3 0.7 dynamic_slice.38
  117.4 1.6 fusion.32
  119.4 6.5 %collective-permute-start = (bf16[30,128]{1,0:T(8,128)(2,1)S(1)}, bf16[30,128]{1,0:T(8,128)(2,1)S(1)}, u32[]{:S(2)}, u32[]{:S(2)}) collective-permute-start(bf16[30,128]{1,0:T(8,128)(2,1)S(1)} %slice.274), channel_id=1, source_target_pairs={{0,4},{4,8},{8,12},{12,16},{16,20},{20,24},{24,28},{1,5},{5,9},{9,... | collective-permute-start | bytes 23048 | tf_op jit(solution)/shard_map/ppermute | solution.py:20
  125.9 0.6 fusion.47
  126.5 0.7 collective-permute-done
  127.9 5.8 %psum.7 = f32[256]{0:T(256)S(1)} all-reduce(f32[256]{0:T(256)S(1)} %get-tuple-element.287), channel_id=1, replica_groups=mesh['sp'=8,'tp'=4] {'tp'}, use_global_device_ids=true, to_apply=%region_2.3 | all-reduce | flops 256 | bytes 2048 | tf_op jit(solution)/shard_map/psum | solution.py:145
  133.7 2.3 %fusion.83 = f32[256,2048]{1,0:T(8,128)S(1)} fusion(bf16[128,2048]{1,0:T(8,128)(2,1)} %param.32, bf16[2048,128]{1,0:T(8,128)(2,1)} %param.26, bf16[256,2048]{1,0:T(8,128)(2,1)} %all-gather.2.cloned.1.call-done, f32[2048]{0:T(1024)S(1)} %convert_element_type.71, f32[256,128]{1,0:T(8,128)S(1)} %get-tuple-element.288, f32[128]{0:T(128)S(1)} %copy-done.3, ...), kind=kOutput, calls=%fused_computation.126 | convolution fusion | flops 270499840 | bytes 4336128 | tf_op jit(solution)/shard_map/dot_general | solution.py:150
  136.0 1.4 fusion.17
  137.4 42.3 %reduce-scatter.2.cloned.1.call-done = bf16[64,2048]{1,0:T(8,128)(2,1)} async-done(((bf16[256,2048]{1,0:T(8,128)(2,1)}), bf16[64,2048]{1,0:T(8,128)(2,1)}) %reduce-scatter.2.cloned.1.call-update) | async-done | bytes 262160 | tf_op jit(solution)/shard_map/reduce_scatter | solution.py:148
  (61 shorter events, 3.3 us)
Async XLA Ops:
  6.5 129.4 %copy-start = (bf16[256,2048]{1,0:T(8,128)(2,1)S(1)}, bf16[256,2048]{1,0:T(8,128)(2,1)}, u32[]{:S(2)}) copy-start(bf16[256,2048]{1,0:T(8,128)(2,1)} %param.33) | copy-start | bytes 3145732
  6.5 21.8 %all-gather.2.cloned.1.call-start = ((), (), s32[]{:S(2)}) async-start(), calls=%async_computation.1 | async-start | bytes 1310720 | tf_op jit(solution)/shard_map/all_gather | solution.py:42
  7.3 172.5 %reduce-scatter.2.cloned.1.call-start = ((), (), s32[]{:S(2)}) async-start(), calls=%async_computation.2 | async-start | bytes 1310720 | tf_op jit(solution)/shard_map/reduce_scatter | solution.py:148
  31.7 37.7 %copy-start.1 = (bf16[256,2048]{1,0:T(8,128)(2,1)S(1)}, bf16[256,2048]{1,0:T(8,128)(2,1)}, u32[]{:S(2)}) copy-start(bf16[256,2048]{1,0:T(8,128)(2,1)} %all-gather.2.cloned.1.call-done) | copy-start | bytes 3145732
  69.4 32.8 %copy-start.5 = (bf16[2048,256]{1,0:T(8,128)(2,1)S(1)}, bf16[2048,256]{1,0:T(8,128)(2,1)}, u32[]{:S(2)}) copy-start(bf16[2048,256]{1,0:T(8,128)(2,1)} %param.23) | copy-start | bytes 3145732
  102.9 13.8 %copy-start.4 = (f32[2]{0:T(128)S(1)}, f32[2]{0:T(128)}, u32[]{:S(2)}) copy-start(f32[2]{0:T(128)} %param.30) | copy-start | bytes 28
  102.9 14.2 %copy-start.2 = (f32[128]{0:T(128)S(1)}, f32[128]{0:T(128)}, u32[]{:S(2)}) copy-start(f32[128]{0:T(128)} %param.31) | copy-start | bytes 1540
  116.7 2.2 %copy-start.7 = (bf16[2048,128]{1,0:T(8,128)(2,1)S(1)}, bf16[2048,128]{1,0:T(8,128)(2,1)}, u32[]{:S(2)}) copy-start(bf16[2048,128]{1,0:T(8,128)(2,1)} %param.21) | copy-start | bytes 1572868
  117.4 8.5 %copy-start.6 = (bf16[2048,256]{1,0:T(8,128)(2,1)S(1)}, bf16[2048,256]{1,0:T(8,128)(2,1)}, u32[]{:S(2)}) copy-start(bf16[2048,256]{1,0:T(8,128)(2,1)} %param.27) | copy-start | bytes 3145732
  119.4 7.8 %collective-permute-start = (bf16[30,128]{1,0:T(8,128)(2,1)S(1)}, bf16[30,128]{1,0:T(8,128)(2,1)S(1)}, u32[]{:S(2)}, u32[]{:S(2)}) collective-permute-start(bf16[30,128]{1,0:T(8,128)(2,1)S(1)} %slice.274), channel_id=1, source_target_pairs={{0,4},{4,8},{8,12},{12,16},{16,20},{20,24},{24,28},{1,5},{5,9},{9,... | collective-permute-start | bytes 23048 | tf_op jit(solution)/shard_map/ppermute | solution.py:20
  127.3 6.4 %copy-start.3 = (f32[128]{0:T(128)S(1)}, f32[128]{0:T(128)}, u32[]{:S(2)}) copy-start(f32[128]{0:T(128)} %param.29) | copy-start | bytes 1540
Sparse Core Ops, SparseCore 0:
  8.9 19.4 all-gather.1
  137.6 42.1 reduce-scatter.1
where the time goes:
time: 187 us
  blocking collectives  70.6 us (38%)
  waiting for transfers between devices  62.3 us (33%)
  between operations  14.2 us (8%)
  matrix products  12 us (6%)
  local copies, waits for them, and re-layouts  10.2 us (5%)
  starting transfers between devices  6.53 us (3%)
  loops' own time  5.83 us (3%)
  other arithmetic  4.96 us (3%)
    reduce_scatter x1, waiting for transfers between devices, local(): lax.psum_scatter((jnp.dot(y_conv, out_conv, preferred_element_type=jnp.fl...  42.3 us
    all_gather x1, blocking collectives, local(): key_piece = lax.all_gather(key, 'sp', axis=0, tiled=True)  33.5 us
    all_gather x1, blocking collectives, local(): value_piece = lax.all_gather(value, 'sp', axis=0, tiled=True)  31.3 us
    all_gather x1, waiting for transfers between devices, local(): lax.all_gather(tokens, 'tp', axis=1, tiled=True).astype(jnp.float32)  18.6 us
    dot_general x6, matrix products, local(): jnp.dot(scaled, weight, preferred_element_type=jnp.float32)  6.52 us
    ppermute x1, starting transfers between devices, shifted(): return lax.ppermute(x, axis, pairs)  6.49 us
    psum x1, blocking collectives, local(): total_sq = lax.psum(jnp.sum(conv * conv, axis=1), 'tp')  5.8 us
    another operation x1, loops' own time, local(): lax.scan(visit, start_attn, (stacked_keys, stacked_values, firsts))  5.67 us
  transfers between devices with their start and end apart: 3, of which 3 were waited for; matrix products, arithmetic and copies ran while one was open for 1% of the time, Pallas kernels for 0%

commit v1 on v0

--- a/solution.py
+++ b/solution.py
@@ -1,3 +1,4 @@
+import functools
 import math
 import jax
 import jax.numpy as jnp
@@ -12,6 +13,23 @@
 EPSILON = 1e-06
 NEG_BIG = -1e30
 HEAD_SCALE = 0.8
+
+
+def remake_the_frame(sample, dim_i):
+    axis_n = lax.axis_size("sp")
+    m_next = sample
+    next_value = sorted(((s, (s + 1) % axis_n) for s in range(axis_n)))
+    shelf = [m_next]
+    for dev_j in range(1, axis_n):
+        m_next = lax.ppermute(m_next, "sp", next_value)
+        shelf.insert(0, m_next)
+    f_next = jnp.concatenate(shelf, axis=dim_i)
+    then = lax.axis_index("sp") + 1
+    reply = jnp.roll(f_next, then * sample.shape[dim_i], axis=dim_i)
+    return reply
+
+
+draw_skins = functools.partial(remake_the_frame, dim_i=0)
 
 
 def shifted(x, axis, by):
@@ -78,7 +96,7 @@
             for rows_of, unused_pos in query_groups
         )
     )
-    key_piece = lax.all_gather(key, "sp", axis=0, tiled=True)
+    key_piece = draw_skins(key)
     value_piece = lax.all_gather(value, "sp", axis=0, tiled=True)
     shards = key_piece.shape[0] // tok_rows
     stacked_keys = key_piece.reshape(shards, tok_rows, kv_local, 2, QK)

time: 187 us -> 168 us (0.90)
  blocking collectives: 70.6 us -> 37.2 us
  waiting for transfers between devices: 62.3 us -> 76.8 us
  local copies, waits for them, and re-layouts: 10.2 us -> 8.16 us
    all_gather x1 -> x0, blocking collectives: 33.5 us -> none  [local(): key_piece = lax.all_gather(key, 'sp', axis=0, tiled=True)]
    ppermute x0 -> x7, waiting for transfers between devices: none -> 22.2 us  [remake_the_frame(): m_next = lax.ppermute(m_next, 'sp', next_value)]
    reduce_scatter x1, waiting for transfers between devices: 42.3 us -> 35.4 us  [local(): lax.psum_scatter((jnp.dot(y_conv, out_conv, preferred_element_type=jnp.fl...]
    ppermute x0 -> x7, starting transfers between devices: none -> 4.76 us  [remake_the_frame(): m_next = lax.ppermute(m_next, 'sp', next_value)]
    ppermute x1, starting transfers between devices: 6.49 us -> 3.38 us  [shifted(): return lax.ppermute(x, axis, pairs)]
    reshape x1, local copies, waits for them, and re-layouts: 2.45 us -> 0.4 us  [local(): stacked_keys = key_piece.reshape(shards, tok_rows, kv_local, 2, QK)]
  transfers between devices with their start and end apart: 3 -> 10, of which waited for: 3 -> 8; matrix products, arithmetic and copies ran while one was open for 1% -> 5% of each run, Pallas kernels for 0% -> 0%
where the time goes in v1:
time: 168 us; the launch traced here: 167 us
  waiting for transfers between devices  76.8 us (46%)
  blocking collectives  37.2 us (22%)
  between operations  14.3 us (9%)
  matrix products  11.5 us (7%)
  starting transfers between devices  8.18 us (5%)
  local copies, waits for them, and re-layouts  8.16 us (5%)
  loops' own time  5.94 us (4%)
  other arithmetic  5.04 us (3%)
    reduce_scatter x1, waiting for transfers between devices, local(): lax.psum_scatter((jnp.dot(y_conv, out_conv, preferred_element_type=jnp.fl...  35.4 us
    all_gather x1, blocking collectives, local(): value_piece = lax.all_gather(value, 'sp', axis=0, tiled=True)  31.4 us
    ppermute x7, waiting for transfers between devices, remake_the_frame(): m_next = lax.ppermute(m_next, 'sp', next_value)  22.2 us
    all_gather x1, waiting for transfers between devices, local(): lax.all_gather(tokens, 'tp', axis=1, tiled=True).astype(jnp.float32)  18.5 us
    dot_general x6, matrix products, local(): jnp.dot(scaled, weight, preferred_element_type=jnp.float32)  5.87 us
    psum x1, blocking collectives, local(): total_sq = lax.psum(jnp.sum(conv * conv, axis=1), 'tp')  5.85 us
    another operation x1, loops' own time, local(): lax.scan(visit, start_attn, (stacked_keys, stacked_values, firsts))  5.78 us
    dynamic_slice x8, local copies, waits for them, and re-layouts, local(): lax.scan(visit, start_attn, (stacked_keys, stacked_values, firsts))  5.35 us
  transfers between devices with their start and end apart: 10, of which 8 were waited for; matrix products, arithmetic and copies ran while one was open for 5% of the time, Pallas kernels for 0%

profile of v1, /device:TPU:0, one launch (start us, length us, event | category | flops | bytes accessed | tf_op | source)
XLA Modules:
  0.0 167.2 jit_solution(10132876171140507593)
XLA Ops:
  6.5 0.7 all-gather.2.cloned.1.call-update
  7.3 0.7 convert_element_type.71
  8.5 0.7 convert_element_type.79
  9.8 18.5 %all-gather.2.cloned.1.call-done = bf16[256,2048]{1,0:T(8,128)(2,1)} async-done(((bf16[256,512]{1,0:T(8,128)(2,1)}), bf16[256,2048]{1,0:T(8,128)(2,1)}) %all-gather.2.cloned.1.call-update) | async-done | bytes 1048592 | tf_op jit(solution)/shard_map/all_gather | solution.py:60
  28.4 1.6 fusion.19
  30.0 1.8 %fusion.35 = bf16[256,128]{1,0:T(8,128)(2,1)S(1)} fusion(bf16[2048,128]{1,0:T(8,128)(2,1)} %param.24, bf16[256,2048]{1,0:T(8,128)(2,1)} %all-gather.2.cloned.1.call-done, f32[2048]{0:T(1024)S(1)} %convert_element_type.71, f32[256]{0:T(256)S(1)} %add_rsqrt_fusion.2), kind=kOutput, calls=%fused_computation.53 | convolution fusion | flops 135856128 | bytes 1647616 | tf_op jit(solution)/shard_map/dot_general | solution.py:64
  31.8 1.5 collective-permute-start.1
  34.3 3.4 %collective-permute-start = (bf16[30,128]{1,0:T(8,128)(2,1)S(1)}, bf16[30,128]{1,0:T(8,128)(2,1)S(1)}, u32[]{:S(2)}, u32[]{:S(2)}) collective-permute-start(bf16[30,128]{1,0:T(8,128)(2,1)S(1)} %slice.274), channel_id=1, source_target_pairs={{0,4},{4,8},{8,12},{12,16},{16,20},{20,24},{24,28},{1,5},{5,9},{9,... | collective-permute-start | bytes 23048 | tf_op jit(solution)/shard_map/ppermute | solution.py:38
  38.9 0.9 collective-permute-start.2
  40.2 5.6 %collective-permute-done.2 = bf16[256,128]{1,0:T(8,128)(2,1)S(1)} collective-permute-done((bf16[256,128]{1,0:T(8,128)(2,1)S(1)}, bf16[256,128]{1,0:T(8,128)(2,1)S(1)}, u32[]{:S(2)}, u32[]{:S(2)}) %collective-permute-start.2) | collective-permute-done | bytes 65568 | tf_op jit(solution)/shard_map/ppermute | solution.py:24
  45.8 31.4 %all_gather.7 = bf16[2048,128]{1,0:T(8,128)(2,1)S(1)} all-gather(bf16[256,128]{1,0:T(8,128)(2,1)S(1)} %fusion.36), channel_id=1, replica_groups=mesh['sp'=8,'tp'=4] {'sp'}, dimensions={0}, use_global_device_ids=true | all-gather | bytes 589824 | tf_op jit(solution)/shard_map/all_gather | solution.py:100
  77.2 2.3 %collective-permute-start.4 = (bf16[256,128]{1,0:T(8,128)(2,1)S(1)}, bf16[256,128]{1,0:T(8,128)(2,1)S(1)}, u32[]{:S(2)}, u32[]{:S(2)}) collective-permute-start(bf16[256,128]{1,0:T(8,128)(2,1)S(1)} %collective-permute-done.3), channel_id=1, source_target_pairs={{0,4},{4,8},{8,12},{12,16},{16,20},{20,24},{24,28},{28,0},{1,5},{5... | collective-permute-start | bytes 196616 | tf_op jit(solution)/shard_map/ppermute | solution.py:24
  79.5 4.8 %collective-permute-done.4 = bf16[256,128]{1,0:T(8,128)(2,1)S(1)} collective-permute-done((bf16[256,128]{1,0:T(8,128)(2,1)S(1)}, bf16[256,128]{1,0:T(8,128)(2,1)S(1)}, u32[]{:S(2)}, u32[]{:S(2)}) %collective-permute-start.4) | collective-permute-done | bytes 65568 | tf_op jit(solution)/shard_map/ppermute | solution.py:24
  84.9 5.8 %psum.7 = f32[256]{0:T(256)S(1)} all-reduce(f32[256]{0:T(256)S(1)} %get-tuple-element.287), channel_id=1, replica_groups=mesh['sp'=8,'tp'=4] {'tp'}, use_global_device_ids=true, to_apply=%region_2.3 | all-reduce | flops 256 | bytes 2048 | tf_op jit(solution)/shard_map/psum | solution.py:163
  91.3 7.0 %collective-permute-done.6 = bf16[256,128]{1,0:T(8,128)(2,1)S(1)} collective-permute-done((bf16[256,128]{1,0:T(8,128)(2,1)S(1)}, bf16[256,128]{1,0:T(8,128)(2,1)S(1)}, u32[]{:S(2)}, u32[]{:S(2)}) %collective-permute-start.6) | collective-permute-done | bytes 65568 | tf_op jit(solution)/shard_map/ppermute | solution.py:24
  98.3 3.3 %fusion.83 = f32[256,2048]{1,0:T(8,128)} fusion(bf16[128,2048]{1,0:T(8,128)(2,1)} %param.32, bf16[2048,128]{1,0:T(8,128)(2,1)} %param.26, bf16[256,2048]{1,0:T(8,128)(2,1)S(1)} %copy-done.2, f32[2048]{0:T(1024)S(1)} %convert_element_type.71, f32[256,128]{1,0:T(8,128)S(1)} %get-tuple-element.288, f32[128]{0:T(128)S(1)} %copy-done.3, ...), kind=kOutput, calls=%fused_computation.126 | convolution fusion | flops 270499840 | bytes 4336128 | tf_op jit(solution)/shard_map/dot_general | solution.py:168
  101.6 3.6 %collective-permute-done.7 = bf16[256,128]{1,0:T(8,128)(2,1)S(1)} collective-permute-done((bf16[256,128]{1,0:T(8,128)(2,1)S(1)}, bf16[256,128]{1,0:T(8,128)(2,1)S(1)}, u32[]{:S(2)}, u32[]{:S(2)}) %collective-permute-start.7) | collective-permute-done | bytes 65568 | tf_op jit(solution)/shard_map/ppermute | solution.py:24
  106.7 13.2 %while.17 = (s32[]{:T(128)}, f32[1,2,2,256]{3,1,2,0:T(2,128)S(1)}, f32[1,2,2,256]{3,1,2,0:T(2,128)S(1)}, f32[1,2,2,256,128]{4,3,2,1,0:T(8,128)S(1)}, s32[8]{0:T(...) while((s32[]{:T(128)}, f32[1,2,2,256]{3,1,2,0:T(2,128)S(1)}, ...), condition=%wide.region_8.9_spmd.clone, body=%wide.region_3.8_spmd.clone.sunk | while | flops 102567424 | bytes 4664615 | solution.py:144
  106.8 0.7 dynamic_slice.44
  108.1 2.0 %conditional.3 = ((f32[1,2,2,256]{3,1,2,0:T(2,128)S(1)}, f32[1,2,2,256]{3,1,2,0:T(2,128)S(1)}, f32[1,2,2,256,128]{4,3,2,1,0:T(8,128)S(1)})) conditional(s32[]{:T(128)} %convert_element_type.190, (f32[1,2,2,256]{3,1,2,0:T(2,128)S(1)}, f32[1,2,2,256]{3,1,2,0:T(2,128)S(1)}, f32[1,2,2,256,128]{4,3,2,1,0:T(8,128)S(1)}) %tuple.82, (s32[]{:T(128)}, ...), branch_computations={%region_4.4_spmd, %region_5.7_spmd} | conditional | flops 102567424 | bytes 4663344 | solution.py:141
  108.1 0.7 broadcast_add_fusion
  110.1 0.7 dynamic_slice.44
  111.5 0.7 dynamic_slice.44
  112.9 0.7 dynamic_slice.44
  114.3 0.7 dynamic_slice.44
  115.7 0.7 dynamic_slice.44
  117.1 0.7 dynamic_slice.44
  118.6 0.7 dynamic_slice.44
  120.5 0.8 copy.30
  121.3 2.2 %fusion.47 = bf16[256,256]{0,1:T(8,128)(2,1)S(1)} fusion(f32[256,1,2,128]{0,3,2,1:T(8,128)} %copy.30, bf16[2048,256]{1,0:T(8,128)(2,1)} %param.27, bf16[256,2048]{1,0:T(8,128)(2,1)} %all-gather.2.cloned.1.call-done, f32[2048]{0:T(1024)S(1)} %convert_element_type.71, f32[256]{0:T(256)S(1)} %add_rsqrt_fusion.2), kind=kOutput, calls=%fused_computation.60 | convolution fusion | flops 270598144 | bytes 2499584 | tf_op jit(solution)/shard_map/dot_general | solution.py:64
  123.5 1.4 fusion.17
  125.0 35.4 %reduce-scatter.2.cloned.1.call-done = bf16[64,2048]{1,0:T(8,128)(2,1)} async-done(((bf16[256,2048]{1,0:T(8,128)(2,1)}), bf16[64,2048]{1,0:T(8,128)(2,1)}) %reduce-scatter.2.cloned.1.call-update) | async-done | bytes 262160 | tf_op jit(solution)/shard_map/reduce_scatter | solution.py:166
  (95 shorter events, 7.4 us)
Async XLA Ops:
  6.5 116.9 %copy-start = (bf16[256,2048]{1,0:T(8,128)(2,1)S(1)}, bf16[256,2048]{1,0:T(8,128)(2,1)}, u32[]{:S(2)}) copy-start(bf16[256,2048]{1,0:T(8,128)(2,1)} %param.33) | copy-start | bytes 3145732
  6.5 26.8 %copy-start.7 = (bf16[2048,128]{1,0:T(8,128)(2,1)S(1)}, bf16[2048,128]{1,0:T(8,128)(2,1)}, u32[]{:S(2)}) copy-start(bf16[2048,128]{1,0:T(8,128)(2,1)} %param.22) | copy-start | bytes 1572868
  6.5 21.8 %all-gather.2.cloned.1.call-start = ((), (), s32[]{:S(2)}) async-start(), calls=%async_computation.1 | async-start | bytes 1310720 | tf_op jit(solution)/shard_map/all_gather | solution.py:60
  7.3 153.1 %reduce-scatter.2.cloned.1.call-start = ((), (), s32[]{:S(2)}) async-start(), calls=%async_computation.2 | async-start | bytes 1310720 | tf_op jit(solution)/shard_map/reduce_scatter | solution.py:166
  28.4 5.0 %copy-start.2 = (bf16[256,2048]{1,0:T(8,128)(2,1)S(1)}, bf16[256,2048]{1,0:T(8,128)(2,1)}, u32[]{:S(2)}) copy-start(bf16[256,2048]{1,0:T(8,128)(2,1)} %all-gather.2.cloned.1.call-done) | copy-start | bytes 3145732
  30.0 3.8 %copy-start.8 = (bf16[2048,128]{1,0:T(8,128)(2,1)S(1)}, bf16[2048,128]{1,0:T(8,128)(2,1)}, u32[]{:S(2)}) copy-start(bf16[2048,128]{1,0:T(8,128)(2,1)} %param.21) | copy-start | bytes 1572868
  31.8 5.8 %copy-start.6 = (bf16[2048,256]{1,0:T(8,128)(2,1)S(1)}, bf16[2048,256]{1,0:T(8,128)(2,1)}, u32[]{:S(2)}) copy-start(bf16[2048,256]{1,0:T(8,128)(2,1)} %param.23) | copy-start | bytes 3145732
  31.8 7.0 %collective-permute-start.1 = (bf16[256,128]{1,0:T(8,128)(2,1)S(1)}, bf16[256,128]{1,0:T(8,128)(2,1)S(1)}, u32[]{:S(2)}, u32[]{:S(2)}) collective-permute-start(bf16[256,128]{1,0:T(8,128)(2,1)S(1)} %fusion.35), channel_id=1, source_target_pairs={{0,4},{4,8},{8,12},{12,16},{16,20},{20,24},{24,28},{28,0},{1,5},{5... | collective-permute-start | bytes 196616 | tf_op jit(solution)/shard_map/ppermute | solution.py:24
  33.8 6.0 %copy-start.9 = (bf16[2048,128]{1,0:T(8,128)(2,1)S(1)}, bf16[2048,128]{1,0:T(8,128)(2,1)}, u32[]{:S(2)}) copy-start(bf16[2048,128]{1,0:T(8,128)(2,1)} %param.25) | copy-start | bytes 1572868
  34.3 45.3 %collective-permute-start = (bf16[30,128]{1,0:T(8,128)(2,1)S(1)}, bf16[30,128]{1,0:T(8,128)(2,1)S(1)}, u32[]{:S(2)}, u32[]{:S(2)}) collective-permute-start(bf16[30,128]{1,0:T(8,128)(2,1)S(1)} %slice.274), channel_id=1, source_target_pairs={{0,4},{4,8},{8,12},{12,16},{16,20},{20,24},{24,28},{1,5},{5,9},{9,... | collective-permute-start | bytes 23048 | tf_op jit(solution)/shard_map/ppermute | solution.py:38
  38.9 7.0 %collective-permute-start.2 = (bf16[256,128]{1,0:T(8,128)(2,1)S(1)}, bf16[256,128]{1,0:T(8,128)(2,1)S(1)}, u32[]{:S(2)}, u32[]{:S(2)}) collective-permute-start(bf16[256,128]{1,0:T(8,128)(2,1)S(1)} %collective-permute-done.1), channel_id=1, source_target_pairs={{0,4},{4,8},{8,12},{12,16},{16,20},{20,24},{24,28},{28,0},{1,5},{5... | collective-permute-start | bytes 196616 | tf_op jit(solution)/shard_map/ppermute | solution.py:24
  45.8 31.4 %collective-permute-start.3 = (bf16[256,128]{1,0:T(8,128)(2,1)S(1)}, bf16[256,128]{1,0:T(8,128)(2,1)S(1)}, u32[]{:S(2)}, u32[]{:S(2)}) collective-permute-start(bf16[256,128]{1,0:T(8,128)(2,1)S(1)} %collective-permute-done.2), channel_id=1, source_target_pairs={{0,4},{4,8},{8,12},{12,16},{16,20},{20,24},{24,28},{28,0},{1,5},{5... | collective-permute-start | bytes 196616 | tf_op jit(solution)/shard_map/ppermute | solution.py:24
  77.2 7.1 %collective-permute-start.4 = (bf16[256,128]{1,0:T(8,128)(2,1)S(1)}, bf16[256,128]{1,0:T(8,128)(2,1)S(1)}, u32[]{:S(2)}, u32[]{:S(2)}) collective-permute-start(bf16[256,128]{1,0:T(8,128)(2,1)S(1)} %collective-permute-done.3), channel_id=1, source_target_pairs={{0,4},{4,8},{8,12},{12,16},{16,20},{20,24},{24,28},{28,0},{1,5},{5... | collective-permute-start | bytes 196616 | tf_op jit(solution)/shard_map/ppermute | solution.py:24
  84.4 7.0 %collective-permute-start.5 = (bf16[256,128]{1,0:T(8,128)(2,1)S(1)}, bf16[256,128]{1,0:T(8,128)(2,1)S(1)}, u32[]{:S(2)}, u32[]{:S(2)}) collective-permute-start(bf16[256,128]{1,0:T(8,128)(2,1)S(1)} %collective-permute-done.4), channel_id=1, source_target_pairs={{0,4},{4,8},{8,12},{12,16},{16,20},{20,24},{24,28},{28,0},{1,5},{5... | collective-permute-start | bytes 196616 | tf_op jit(solution)/shard_map/ppermute | solution.py:24
  84.4 13.9 %copy-start.3 = (f32[128]{0:T(128)S(1)}, f32[128]{0:T(128)}, u32[]{:S(2)}) copy-start(f32[128]{0:T(128)} %param.29) | copy-start | bytes 1540
  91.3 7.0 %collective-permute-start.6 = (bf16[256,128]{1,0:T(8,128)(2,1)S(1)}, bf16[256,128]{1,0:T(8,128)(2,1)S(1)}, u32[]{:S(2)}, u32[]{:S(2)}) collective-permute-start(bf16[256,128]{1,0:T(8,128)(2,1)S(1)} %collective-permute-done.5), channel_id=1, source_target_pairs={{0,4},{4,8},{8,12},{12,16},{16,20},{20,24},{24,28},{28,0},{1,5},{5... | collective-permute-start | bytes 196616 | tf_op jit(solution)/shard_map/ppermute | solution.py:24
  98.3 7.0 %collective-permute-start.7 = (bf16[256,128]{1,0:T(8,128)(2,1)S(1)}, bf16[256,128]{1,0:T(8,128)(2,1)S(1)}, u32[]{:S(2)}, u32[]{:S(2)}) collective-permute-start(bf16[256,128]{1,0:T(8,128)(2,1)S(1)} %collective-permute-done.6), channel_id=1, source_target_pairs={{0,4},{4,8},{8,12},{12,16},{16,20},{20,24},{24,28},{28,0},{1,5},{5... | collective-permute-start | bytes 196616 | tf_op jit(solution)/shard_map/ppermute | solution.py:24
  106.7 13.2 %copy-start.5 = (f32[2]{0:T(128)S(1)}, f32[2]{0:T(128)}, u32[]{:S(2)}) copy-start(f32[2]{0:T(128)} %param.30) | copy-start | bytes 28
  106.7 13.6 %copy-start.4 = (f32[128]{0:T(128)S(1)}, f32[128]{0:T(128)}, u32[]{:S(2)}) copy-start(f32[128]{0:T(128)} %param.31) | copy-start | bytes 1540
  120.5 3.0 %copy-start.1 = (f32[256,2048]{1,0:T(8,128)S(1)}, f32[256,2048]{1,0:T(8,128)}, u32[]{:S(2)}) copy-start(f32[256,2048]{1,0:T(8,128)} %fusion.83) | copy-start | bytes 6291460
Sparse Core Ops, SparseCore 0:
  8.9 19.4 all-gather.1
  125.1 35.2 reduce-scatter.1
